TPU v7x, 256 devices: a 4x2x16 block of a 4x16x16 slice. The times are simulated.
256 devices in a mesh: grp: 2 (over y), sp: 16 (over z), tp: 8 (over x, core).
Axes of the slice: x: 4, y: 2, z: 16, core: 2. Of those that a mesh axis runs over, the one named last changes fastest.
The devices are a block of a 4x16x16 slice.
Arguments:
- tokens: bfloat16 [16384, 4096], P(('grp', 'sp', 'tp')), parts along dimension 0, may hold values from -6 to 6
- norm_gain: float32 [4096], replicated, may hold values from 0.1 to 1.9
- query_diff: bfloat16 [4096, 2048], P('sp', 'tp'), may hold values from -1.25 to 1.25
- key_diff: bfloat16 [4096, 2048], P('sp', 'tp'), may hold values from -1.25 to 1.25
- value_diff: bfloat16 [4096, 2048], P('sp', 'tp'), may hold values from -0.09375 to 0.09375
- lam: float32 [8], P('tp'), may hold values from 0.3 to 0.8
- output_norm_gain: float32 [256], replicated, may hold values from 0.1 to 1.9
- query_win: bfloat16 [4096, 2048], P('sp', 'tp'), may hold values from -1.25 to 1.25
- keyval_win: bfloat16 [4, 4096, 256], P(None, 'sp'), may hold values from -1.25 to 1.25
- sink: float32 [16], P('tp'), may hold values from 4 to 7
- proj_diff: bfloat16 [2048, 4096], P('tp'), may hold values from -0.125 to 0.125
- proj_win: bfloat16 [2048, 4096], P('tp'), may hold values from -0.79296875 to 0.79296875
Outputs:
- mixed: bfloat16 [16384, 4096], P(('grp', 'sp', 'tp')), parts along dimension 0
There are 2 independent parts, one for each index of `grp`. A program takes and returns all parts, laid end to end along the dimension named above; an argument that names none is the same for every part. Nothing has to cross between parts.
All inputs are finite; a program needn't handle non-finite values.
Results may differ from a plain program's by a relative error of at most 0.015.
Values may be sent and summed in bfloat16 or wider, within the bound.
A program may use at most 128 MiB of HBM per device.

v0:
```python
import math
import jax
import jax.numpy as jnp
from jax import lax
from jax.sharding import Mesh
from jax.sharding import PartitionSpec as P

HEAD = 128
WIN_HEADS = 16
KV_HEADS = 4
WINDOW = 128
VDIM = 256
TP = ("tp_0", "tp_1")
GRP_SP_TP = ("grp", "sp", "tp_0", "tp_1")
EPS = 1e-06


def in_order(parts, dim):
    shape = list(parts.shape[1:])
    shape[dim] *= parts.shape[0]
    return jnp.moveaxis(parts, 0, dim).reshape(shape)


def stacked_from(x, axes, order):
    parts = x[None]
    for k in order:
        parts = lax.all_gather(parts, axes[k], axis=0, tiled=True)
    block = [lax.axis_size(axes[k]) for k in reversed(order)]
    parts = parts.reshape(*block, *x.shape)
    turned = sorted(range(len(order)), key=lambda place: order[len(order) - 1 - place])
    return parts.transpose(*turned, *range(len(order), parts.ndim)).reshape(-1, *x.shape)


def gathered_by_axis(x, axes, order, dim):
    return in_order(stacked_from(x, axes, order), dim)


def side_by_side(arrays, axis, dim, along):
    both = jnp.concatenate(arrays, axis=along)
    out, at, done = (lax.all_gather(both, axis, axis=dim, tiled=True), 0, [])
    for a in arrays:
        done.append(lax.slice_in_dim(out, at, at + a.shape[along], axis=along))
        at += a.shape[along]
    return tuple(done)


def padded_2(x, sides, width):
    for axis, dim in sides:
        devices, length = (lax.axis_size(axis), x.shape[dim])
        up = [(i, (i + 1) % devices) for i in range(devices - 1)]
        down = [(j, i) for i, j in up]
        last = lax.slice_in_dim(x, length - width, length, axis=dim)
        first = lax.slice_in_dim(x, 0, width, axis=dim)
        before = lax.ppermute(last, axis, up)
        after = lax.ppermute(first, axis, down)
        x = jnp.concatenate([before, x, after], axis=dim)
    return x


def root_mean_square_rows(values, gain):
    return values * lax.rsqrt(jnp.mean(values * values, axis=-1, keepdims=True) + EPS) * gain


def body(
    tokens,
    norm_gain,
    query_diff,
    key_diff,
    value_diff,
    lam,
    output_norm_gain,
    query_win,
    keyval_win,
    sink,
    proj_diff,
    proj_win,
):
    normed = root_mean_square_rows(tokens.astype(jnp.float32), norm_gain).astype(jnp.bfloat16)
    heads_diff = lam.shape[0]
    heads_win = sink.shape[0]
    group = WIN_HEADS // KV_HEADS
    kv_index = lax.axis_index(TP) * heads_win // group
    kv_local = lax.dynamic_index_in_dim(keyval_win, kv_index, 0, keepdims=False)
    pieces = [query_diff, key_diff, value_diff, query_win, kv_local]
    stacked = jnp.concatenate(pieces, axis=1)
    rows_all = gathered_by_axis(normed, TP, (0, 1), 0)
    projected = jnp.dot(
        rows_all,
        lax.all_gather(stacked, "sp", axis=0, tiled=True),
        preferred_element_type=jnp.float32,
    )
    projected = projected.astype(jnp.bfloat16)
    output_list = []
    offset = 0
    for piece in pieces:
        output_list.append(projected[:, offset : offset + piece.shape[1]])
        offset = offset + piece.shape[1]
    q_diff, k_diff, v_diff, q_win, kv_win = output_list
    tok = projected.shape[0]
    scale = HEAD ** (-0.5)
    q_four = q_diff.reshape(tok, heads_diff, 2, HEAD)
    start_state = (
        jnp.full((heads_diff, 2, tok), -jnp.inf, jnp.float32),
        jnp.zeros((heads_diff, 2, tok), jnp.float32),
        jnp.zeros((heads_diff, 2, tok, VDIM), jnp.float32),
    )
    carry = start_state
    keys, values = side_by_side((k_diff, v_diff), "sp", 0, 1)
    rows = keys.shape[0]
    step = math.gcd(rows, 1024)
    key_blocks = keys.reshape(rows // step, step, heads_diff, 2, HEAD)
    value_blocks = values.reshape(rows // step, step, heads_diff, VDIM)

    def one(state, block):
        top, total, acc = state
        key_part, value_part = block
        scores = (
            jnp.einsum("qhmd,khmd->hmqk", q_four, key_part, preferred_element_type=jnp.float32)
            * scale
        )
        new_top = jnp.maximum(top, jnp.max(scores, axis=-1))
        expo = jnp.exp(scores - new_top[..., None])
        fade = jnp.exp(top - new_top)
        total = total * fade + jnp.sum(expo, axis=-1)
        acc = acc * fade[..., None] + jnp.einsum(
            "hmqk,khe->hmqe",
            expo.astype(jnp.bfloat16),
            value_part,
            preferred_element_type=jnp.float32,
        )
        return ((new_top, total, acc), None)

    carry, unused = lax.scan(one, carry, (key_blocks, value_blocks))
    top, total, acc = carry
    attention_maps = acc / total[..., None]
    difference_output = attention_maps[:, 0] - lam[:, None, None] * attention_maps[:, 1]
    differential_output = root_mean_square_rows(difference_output, output_norm_gain).astype(
        jnp.bfloat16
    )
    differential_output = jnp.transpose(differential_output, (1, 0, 2)).reshape(
        tok, heads_diff * VDIM
    )
    padded = padded_2(kv_win, (("sp", 0),), WINDOW)
    nblocks = tok // WINDOW
    blocks = padded.reshape(nblocks + 2, WINDOW, 2 * HEAD)
    band = jnp.concatenate([blocks[:-2], blocks[1:-1], blocks[2:]], axis=1)
    q_blocks = q_win.reshape(nblocks, WINDOW, heads_win, HEAD)
    scores = (
        jnp.einsum("nqhd,nkd->nhqk", q_blocks, band[..., :HEAD], preferred_element_type=jnp.float32)
        * scale
    )
    q_index = jnp.arange(WINDOW)
    k_index = jnp.arange(3 * WINDOW)
    relative = k_index[None, :] - WINDOW - q_index[:, None]
    first_key = lax.axis_index("sp") * tok - WINDOW
    key_pos = first_key + jnp.arange(nblocks)[:, None] * WINDOW + k_index[None, :]
    inside = (key_pos >= 0) & (key_pos < tok * lax.axis_size("sp"))
    valid = (jnp.abs(relative) <= WINDOW)[None] & inside[:, None, :]
    scores = jnp.where(valid[:, None], scores, -jnp.inf)
    sink_logit = sink[None, :, None, None]
    top_win = jnp.maximum(jnp.max(scores, axis=-1, keepdims=True), sink_logit)
    expo = jnp.exp(scores - top_win)
    weights = expo / (jnp.sum(expo, axis=-1, keepdims=True) + jnp.exp(sink_logit - top_win))
    y_win = jnp.einsum(
        "nhqk,nkd->nqhd",
        weights.astype(jnp.bfloat16),
        band[..., HEAD:],
        preferred_element_type=jnp.float32,
    ).astype(jnp.bfloat16)
    y_win = y_win.reshape(tok, heads_win * HEAD)
    summed = jnp.dot(differential_output, proj_diff, preferred_element_type=jnp.float32)
    return lax.psum_scatter(
        (summed + jnp.dot(y_win, proj_win, preferred_element_type=jnp.float32)).astype(
            jnp.bfloat16
        ),
        TP,
        scatter_dimension=0,
        tiled=True,
    )


def solution(mesh):
    torus = Mesh(
        mesh.devices.reshape(mesh.shape["grp"], mesh.shape["sp"], 4, 2),
        ("grp", "sp", "tp_0", "tp_1"),
    )
    return jax.shard_map(
        body,
        mesh=torus,
        in_specs=(
            P(GRP_SP_TP, None),
            P(),
            P("sp", TP),
            P("sp", TP),
            P("sp", TP),
            P(TP),
            P(),
            P("sp", TP),
            P(None, "sp", None),
            P(TP),
            P(TP, None),
            P(TP, None),
        ),
        out_specs=P(GRP_SP_TP, None),
        check_vma=False,
    )
```

profile of v0, /device:TPU:40, one launch (start us, length us, event | category | flops | bytes accessed | tf_op | source)
XLA Modules:
  0.0 442.2 jit_solution(13832787000681153917)
XLA Ops:
  8.0 2.0 fusion.24
  10.2 50.1 %all-gather.12.cloned.1.call-done = bf16[256,4096]{1,0:T(8,128)(2,1)} async-done(((bf16[64,4096]{1,0:T(8,128)(2,1)}), bf16[256,4096]{1,0:T(8,128)(2,1)}) %all-gather.12.cloned.1.call-update) | async-done | bytes 2097168 | tf_op jit(solution)/shard_map/all_gather | solution.py:27
  62.5 22.3 %all-gather.6.cloned.1.call-done = bf16[8,64,4096]{2,1,0:T(8,128)(2,1)} async-done(((bf16[4,64,4096]{2,1,0:T(8,128)(2,1)}), bf16[8,64,4096]{2,1,0:T(8,128)(2,1)}) %all-gather.6.cloned.1.call-update) | async-done | bytes 4194320 | tf_op jit(solution)/shard_map/all_gather | solution.py:27
  84.8 4.7 %copy.38 = bf16[4,2,64,4096]{3,2,1,0:T(8,128)(2,1)} copy(bf16[4,2,64,4096]{3,2,0,1:T(8,128)(2,1)} %bitcast.110) | data formatting | bytes 8388608 | tf_op jit(solution)/shard_map/transpose | solution.py:31
  89.5 123.6 %all-gather.8.cloned.1.call-done = bf16[4096,1280]{1,0:T(8,128)(2,1)} async-done(((bf16[256,1280]{1,0:T(8,128)(2,1)}), bf16[4096,1280]{1,0:T(8,128)(2,1)}) %all-gather.8.cloned.1.call-update) | async-done | bytes 10485776 | tf_op jit(solution)/shard_map/all_gather | solution.py:89
  213.0 10.4 %convolution_convert_fusion = bf16[512,1280]{1,0:T(8,128)(2,1)S(1)} fusion(bf16[512,4096]{1,0:T(8,128)(2,1)} %bitcast.111, bf16[4096,1280]{1,0:T(8,128)(2,1)} %all-gather.8.cloned.1.call-done), kind=kOutput, calls=%fused_computation.26 | convolution fusion | flops 5369364480 | bytes 15990784 | tf_op jit(solution)/shard_map/dot_general | solution.py:87
  227.0 1.4 collective-permute-start
  228.4 1.5 collective-permute-start.1
  231.3 3.5 collective-permute-done.1
  236.4 90.3 %all-gather.10.cloned.1.call-done = bf16[8192,512]{1,0:T(8,128)(2,1)} async-done(((bf16[512,512]{1,0:T(8,128)(2,1)}), bf16[8192,512]{1,0:T(8,128)(2,1)}) %all-gather.10.cloned.1.call-update) | async-done | bytes 8388624 | tf_op jit(solution)/shard_map/all_gather | solution.py:40
  326.7 5.7 %fusion.39 = (bf16[8192,256]{1,0:T(8,128)(2,1)}, bf16[8192,256]{1,0:T(8,128)(2,1)}) fusion(bf16[8192,512]{1,0:T(8,128)(2,1)} %all-gather.10.cloned.1.call-done), kind=kLoop, calls=%fused_computation.73 | loop fusion | bytes 16777216 | tf_op jit(solution)/shard_map/slice | solution.py:42
  332.4 6.9 %reshape.210 = bf16[8,1024,1,2,128]{4,3,1,0,2:T(2,128)(2,1)} reshape(bf16[8192,256]{1,0:T(8,128)(2,1)} %get-tuple-element.116) | data formatting | bytes 8388608 | tf_op jit(solution)/shard_map/reshape | solution.py:111
  339.3 47.5 %while.15 = (s32[]{:T(128)}, f32[1,2,512]{2,1,0:T(2,128)S(1)}, f32[1,2,512]{2,1,0:T(2,128)S(1)}, f32[1,2,512,256]{3,2,1,0:T(8,128)}, bf16[8,1024,1,2,128]{4,3,1,...) while((s32[]{:T(128)}, f32[1,2,512]{2,1,0:T(2,128)S(1)}, ...), condition=%wide.region_4.5_spmd.clone, body=%wide.region_1.4_spmd.clone.sunk | while | flops 814487552 | bytes 25493680 | solution.py:133
  342.2 2.1 fusion.56
  348.1 2.1 fusion.56
  354.1 2.1 fusion.56
  360.0 2.1 fusion.56
  365.9 2.1 fusion.56
  371.9 2.1 fusion.56
  377.8 2.1 fusion.56
  383.8 2.1 fusion.56
  386.8 1.4 broadcast_divide_fusion
  390.0 3.3 add_convert_fusion
  393.4 42.3 %reduce-scatter.2.cloned.1.call-done = bf16[64,4096]{1,0:T(8,128)(2,1)} async-done(((bf16[512,4096]{1,0:T(8,128)(2,1)}), bf16[64,4096]{1,0:T(8,128)(2,1)}) %reduce-scatter.2.cloned.1.call-update) | async-done | bytes 524304 | tf_op jit(solution)/shard_map/reduce_scatter | solution.py:172
  (145 shorter events, 41.7 us)
Async XLA Ops:
  6.5 381.9 %copy-start = (bf16[256,4096]{1,0:T(8,128)(2,1)S(1)}, bf16[256,4096]{1,0:T(8,128)(2,1)}, u32[]{:S(2)}) copy-start(bf16[256,4096]{1,0:T(8,128)(2,1)} %param.24) | copy-start | bytes 6291460
  6.6 54.0 %copy-start.7 = (bf16[256,256]{1,0:T(8,128)(2,1)S(1)}, bf16[256,256]{1,0:T(8,128)(2,1)}, u32[]{:S(2)}) copy-start(bf16[256,256]{1,0:T(8,128)(2,1)} %param.16) | copy-start | bytes 393220
  6.6 54.0 %copy-start.8 = (bf16[256,256]{1,0:T(8,128)(2,1)S(1)}, bf16[256,256]{1,0:T(8,128)(2,1)}, u32[]{:S(2)}) copy-start(bf16[256,256]{1,0:T(8,128)(2,1)} %param.17) | copy-start | bytes 393220
  6.6 54.0 %copy-start.9 = (bf16[256,256]{1,0:T(8,128)(2,1)S(1)}, bf16[256,256]{1,0:T(8,128)(2,1)}, u32[]{:S(2)}) copy-start(bf16[256,256]{1,0:T(8,128)(2,1)} %param.18) | copy-start | bytes 393220
  6.6 54.0 %copy-start.10 = (bf16[256,256]{1,0:T(8,128)(2,1)S(1)}, bf16[256,256]{1,0:T(8,128)(2,1)}, u32[]{:S(2)}) copy-start(bf16[256,256]{1,0:T(8,128)(2,1)} %param.21) | copy-start | bytes 393220
  6.6 53.8 %all-gather.12.cloned.1.call-start = ((), (), s32[]{:S(2)}) async-start(), calls=%async_computation.5 | async-start | bytes 2621440 | tf_op jit(solution)/shard_map/all_gather | solution.py:27
  10.1 74.7 %all-gather.6.cloned.1.call-start = ((), (), s32[]{:S(2)}) async-start(), calls=%async_computation.1 | async-start | bytes 6291456 | tf_op jit(solution)/shard_map/all_gather | solution.py:27
  60.4 152.6 %all-gather.8.cloned.1.call-start = ((), (), s32[]{:S(2)}) async-start(), calls=%async_computation.2 | async-start | bytes 11141120 | tf_op jit(solution)/shard_map/all_gather | solution.py:89
  62.4 264.2 %all-gather.10.cloned.1.call-start = ((), (), s32[]{:S(2)}) async-start(), calls=%async_computation.3 | async-start | bytes 8912896 | tf_op jit(solution)/shard_map/all_gather | solution.py:40
  223.4 5.0 %copy-start.2 = (bf16[512,1280]{1,0:T(8,128)(2,1)}, bf16[512,1280]{1,0:T(8,128)(2,1)S(1)}, u32[]{:S(2)}) copy-start(bf16[512,1280]{1,0:T(8,128)(2,1)S(1)} %convolution_convert_fusion) | copy-start | bytes 3932164
  224.4 211.3 %reduce-scatter.2.cloned.1.call-start = ((), (), s32[]{:S(2)}) async-start(), calls=%async_computation.4 | async-start | bytes 4718592 | tf_op jit(solution)/shard_map/reduce_scatter | solution.py:172
  227.0 8.3 %copy-start.12 = (f32[2]{0:T(128)S(1)}, f32[2]{0:T(128)}, u32[]{:S(2)}) copy-start(f32[2]{0:T(128)} %param.23) | copy-start | bytes 28
  227.0 4.4 collective-permute-start
  228.4 6.4 %collective-permute-start.1 = (bf16[128,256]{1,0:T(8,128)(2,1)}, bf16[128,256]{1,0:T(8,128)(2,1)S(1)}, u32[]{:S(2)}, u32[]{:S(2)}) collective-permute-start(bf16[128,256]{1,0:T(8,128)(2,1)} %get-tuple-element.121), channel_id=1, source_target_pairs={{8,0},{16,8},{24,16},{32,24},{40,32},{48,40},{56,48},{64,56},{72,6... | collective-permute-start | bytes 196616 | tf_op jit(solution)/shard_map/ppermute | solution.py:55
  229.9 5.0 %copy-start.6 = (pred[4,128,384]{1,2,0:T(8,128)(4,1)S(1)}, pred[4,128,384]{1,2,0:T(8,128)(4,1)}, u32[]{:S(2)}) copy-start(pred[4,128,384]{1,2,0:T(8,128)(4,1)} %broadcast_and_fusion) | copy-start | bytes 589828
  339.3 49.1 %copy-start.11 = (f32[256]{0:T(256)S(1)}, f32[256]{0:T(256)}, u32[]{:S(2)}) copy-start(f32[256]{0:T(256)} %param.20) | copy-start | bytes 3076
  346.7 1.5 copy-start.3
  352.6 1.5 copy-start.3
  358.5 1.5 copy-start.3
  364.5 1.5 copy-start.3
  370.4 1.5 copy-start.3
  376.4 1.5 copy-start.3
  382.3 1.5 copy-start.3
  388.4 1.6 copy-start.1
  (10 other events, 10.2 us)
Sparse Core Ops, SparseCore 0:
  10.3 50.0 all-gather.11
  62.2 22.5 all-gather.5
  86.6 126.3 all-gather.7
  224.5 102.1 all-gather.9
  393.5 42.0 reduce-scatter.1
where the time goes:
time: 443 us; the launch traced here: 442 us
  waiting for transfers between devices  332 us (75%)
  local copies, waits for them, and re-layouts  41.4 us (9%)
  matrix products  38.1 us (9%)
  between operations  14.2 us (3%)
  other arithmetic  12.5 us (3%)
    all_gather x1, waiting for transfers between devices, body(): lax.all_gather(stacked, 'sp', axis=0, tiled=True)  124 us
    all_gather x1, waiting for transfers between devices, side_by_side(): out, at, done = (lax.all_gather(both, axis, axis=dim, tiled=True), 0, [])  90.3 us
    all_gather x2, waiting for transfers between devices, stacked_from(): parts = lax.all_gather(parts, axes[k], axis=0, tiled=True)  72.4 us
    reduce_scatter x1, waiting for transfers between devices, body(): lax.psum_scatter((summed + jnp.dot(y_win, proj_win, preferred_element_typ...  42.3 us
    dot_general x8, matrix products, one(): jnp.einsum('hmqk,khe->hmqe', expo.astype(jnp.bfloat16), value_part, prefe...  16.5 us
    dynamic_slice x8, local copies, waits for them, and re-layouts, body(): carry, unused = lax.scan(one, carry, (key_blocks, value_blocks))  11.2 us
    dot_general x1, matrix products, body(): jnp.dot(rows_all, lax.all_gather(stacked, 'sp', axis=0, tiled=True), pref...  10.4 us
  transfers between devices with their start and end apart: 7, of which 6 were waited for; matrix products, arithmetic and copies ran while one was open for 2% of the time, Pallas kernels for 0%

commit v1 on v0

--- a/solution.py
+++ b/solution.py
@@ -13,6 +13,27 @@
 TP = ("tp_0", "tp_1")
 GRP_SP_TP = ("grp", "sp", "tp_0", "tp_1")
 EPS = 1e-06
+
+
+def collect(x, axis, dim):
+    count, mine, width = (lax.axis_size(axis), lax.axis_index(axis), x.shape[dim])
+    right = [(i, (i + 1) % count) for i in range(count)]
+    backward = [(i, (i - 1) % count) for i in range(count)]
+    out = jnp.zeros((*x.shape[:dim], count * width, *x.shape[dim + 1 :]), x.dtype)
+    out = lax.dynamic_update_slice_in_dim(out, x, mine * width, axis=dim)
+    from_left = from_right = x
+    half = count // 2
+    for step in range(1, half + 1):
+        from_left = lax.ppermute(from_left, axis, right)
+        out = lax.dynamic_update_slice_in_dim(
+            out, from_left, (mine - step) % count * width, axis=dim
+        )
+        if step < count - half:
+            from_right = lax.ppermute(from_right, axis, backward)
+            out = lax.dynamic_update_slice_in_dim(
+                out, from_right, (mine + step) % count * width, axis=dim
+            )
+    return out
 
 
 def in_order(parts, dim):
@@ -84,11 +105,7 @@
     pieces = [query_diff, key_diff, value_diff, query_win, kv_local]
     stacked = jnp.concatenate(pieces, axis=1)
     rows_all = gathered_by_axis(normed, TP, (0, 1), 0)
-    projected = jnp.dot(
-        rows_all,
-        lax.all_gather(stacked, "sp", axis=0, tiled=True),
-        preferred_element_type=jnp.float32,
-    )
+    projected = jnp.dot(rows_all, collect(stacked, "sp", 0), preferred_element_type=jnp.float32)
     projected = projected.astype(jnp.bfloat16)
     output_list = []
     offset = 0

time: 443 us -> 412 us (0.930)
  waiting for transfers between devices: 332 us -> 207 us
  starting transfers between devices: 3.23 us -> 46.6 us
  matrix products: 38.1 us -> 72.7 us
  local copies, waits for them, and re-layouts: 41.4 us -> 57.8 us
    all_gather x1 -> x0, waiting for transfers between devices: 124 us -> none  [body(): lax.all_gather(stacked, 'sp', axis=0, tiled=True)]
    ppermute x0 -> x15, waiting for transfers between devices: none -> 77.6 us  [the longest x8 66.2 us: collect(): from_left = lax.ppermute(from_left, axis, right)]
    all_gather x2, waiting for transfers between devices: 72.4 us -> 0.01 us  [stacked_from(): parts = lax.all_gather(parts, axes[k], axis=0, tiled=True)]
    ppermute x0 -> x15, starting transfers between devices: none -> 43.4 us  [the longest x7 40.5 us: collect(): from_right = lax.ppermute(from_right, axis, backward)]
    dot_general x8, matrix products: 16.5 us -> 37 us  [one(): jnp.einsum('hmqk,khe->hmqe', expo.astype(jnp.bfloat16), value_part, prefe...]
    dynamic_update_slice x0 -> x16, local copies, waits for them, and re-layouts: none -> 18.7 us  [the longest x7 9.49 us: collect(): lax.dynamic_update_slice_in_dim(out, from_right, (mine + step) % count *...]
    dot_general x8, matrix products: 5.78 us -> 21.8 us  [one(): jnp.einsum('qhmd,khmd->hmqk', q_four, key_part, preferred_element_type=jn...]
    all_gather x1, waiting for transfers between devices: 90.3 us -> 82 us  [side_by_side(): out, at, done = (lax.all_gather(both, axis, axis=dim, tiled=True), 0, [])]
  transfers between devices with their start and end apart: 7 -> 21, of which waited for: 6 -> 15; matrix products, arithmetic and copies ran while one was open for 2% -> 8% of each run, Pallas kernels for 0% -> 0%
where the time goes in v1:
time: 412 us; the launch traced here: 411 us
  waiting for transfers between devices  207 us (50%)
  matrix products  72.7 us (18%)
  local copies, waits for them, and re-layouts  57.8 us (14%)
  starting transfers between devices  46.6 us (11%)
  between operations  14.1 us (3%)
  other arithmetic  12.5 us (3%)
    all_gather x1, waiting for transfers between devices, side_by_side(): out, at, done = (lax.all_gather(both, axis, axis=dim, tiled=True), 0, [])  82 us
    ppermute x8, waiting for transfers between devices, collect(): from_left = lax.ppermute(from_left, axis, right)  66.2 us
    reduce_scatter x1, waiting for transfers between devices, body(): lax.psum_scatter((summed + jnp.dot(y_win, proj_win, preferred_element_typ...  42.3 us
    ppermute x7, starting transfers between devices, collect(): from_right = lax.ppermute(from_right, axis, backward)  40.5 us
    dot_general x8, matrix products, one(): jnp.einsum('hmqk,khe->hmqe', expo.astype(jnp.bfloat16), value_part, prefe...  37 us
    dot_general x8, matrix products, one(): jnp.einsum('qhmd,khmd->hmqk', q_four, key_part, preferred_element_type=jn...  21.8 us
    ppermute x7, waiting for transfers between devices, collect(): from_right = lax.ppermute(from_right, axis, backward)  11.4 us
    dynamic_slice x8, local copies, waits for them, and re-layouts, body(): carry, unused = lax.scan(one, carry, (key_blocks, value_blocks))  11.3 us
  transfers between devices with their start and end apart: 21, of which 15 were waited for; matrix products, arithmetic and copies ran while one was open for 8% of the time, Pallas kernels for 0%

profile of v1, /device:TPU:40, one launch (start us, length us, event | category | flops | bytes accessed | tf_op | source)
XLA Modules:
  0.0 410.9 jit_solution(8073102060252744389)
XLA Ops:
  17.6 19.7 %collective-permute-start.1 = (bf16[256,1280]{1,0:T(8,128)(2,1)S(1)}, bf16[256,1280]{1,0:T(8,128)(2,1)}, u32[]{:S(2)}, u32[]{:S(2)}) collective-permute-start(bf16[256,1280]{1,0:T(8,128)(2,1)S(1)} %bitcast_dynamic-update-slice_fusion), channel_id=1, source_target_pairs={{0,120},{8,0},{16,8},{24,16},{32,24},{40,32},{48,40},{56,48},{64,5... | collective-permute-start | bytes 1966088 | tf_op jit(solution)/shard_map/ppermute | solution.py:32
  37.4 14.7 %collective-permute-done = bf16[256,1280]{1,0:T(8,128)(2,1)S(1)} collective-permute-done((bf16[256,1280]{1,0:T(8,128)(2,1)S(1)}, bf16[256,1280]{1,0:T(8,128)(2,1)S(1)}, u32[]{:S(2)}, u32[]{:S(2)}) %collective-permute-start) | collective-permute-done | bytes 655392 | tf_op jit(solution)/shard_map/ppermute | solution.py:27
  55.3 14.1 %collective-permute-done.2 = bf16[256,1280]{1,0:T(8,128)(2,1)} collective-permute-done((bf16[256,1280]{1,0:T(8,128)(2,1)S(1)}, bf16[256,1280]{1,0:T(8,128)(2,1)}, u32[]{:S(2)}, u32[]{:S(2)}) %collective-permute-start.2) | collective-permute-done | bytes 655392 | tf_op jit(solution)/shard_map/ppermute | solution.py:27
  72.9 13.1 %collective-permute-done.4 = bf16[256,1280]{1,0:T(8,128)(2,1)S(1)} collective-permute-done((bf16[256,1280]{1,0:T(8,128)(2,1)}, bf16[256,1280]{1,0:T(8,128)(2,1)S(1)}, u32[]{:S(2)}, u32[]{:S(2)}) %collective-permute-start.4) | collective-permute-done | bytes 655392 | tf_op jit(solution)/shard_map/ppermute | solution.py:27
  86.1 4.7 %broadcast_in_dim.24 = bf16[4096,1280]{1,0:T(8,128)(2,1)} broadcast(bf16[]{:T(256)} %constant.151.clone.1), dimensions={} | broadcast | bytes 10485762 | tf_op jit(solution)/shard_map/broadcast_in_dim | solution.py:22
  112.3 4.3 %collective-permute-done.8 = bf16[256,1280]{1,0:T(8,128)(2,1)S(1)} collective-permute-done((bf16[256,1280]{1,0:T(8,128)(2,1)S(1)}, bf16[256,1280]{1,0:T(8,128)(2,1)S(1)}, u32[]{:S(2)}, u32[]{:S(2)}) %collective-permute-start.8) | collective-permute-done | bytes 655392 | tf_op jit(solution)/shard_map/ppermute | solution.py:27
  127.1 4.4 %collective-permute-done.10 = bf16[256,1280]{1,0:T(8,128)(2,1)S(1)} collective-permute-done((bf16[256,1280]{1,0:T(8,128)(2,1)S(1)}, bf16[256,1280]{1,0:T(8,128)(2,1)S(1)}, u32[]{:S(2)}, u32[]{:S(2)}) %collective-permute-start.10) | collective-permute-done | bytes 655392 | tf_op jit(solution)/shard_map/ppermute | solution.py:27
  142.0 4.4 %collective-permute-done.12 = bf16[256,1280]{1,0:T(8,128)(2,1)S(1)} collective-permute-done((bf16[256,1280]{1,0:T(8,128)(2,1)S(1)}, bf16[256,1280]{1,0:T(8,128)(2,1)S(1)}, u32[]{:S(2)}, u32[]{:S(2)}) %collective-permute-start.12) | collective-permute-done | bytes 655392 | tf_op jit(solution)/shard_map/ppermute | solution.py:27
  151.0 7.4 %collective-permute-done.14 = bf16[256,1280]{1,0:T(8,128)(2,1)S(1)} collective-permute-done((bf16[256,1280]{1,0:T(8,128)(2,1)S(1)}, bf16[256,1280]{1,0:T(8,128)(2,1)S(1)}, u32[]{:S(2)}, u32[]{:S(2)}) %collective-permute-start.14) | collective-permute-done | bytes 655392 | tf_op jit(solution)/shard_map/ppermute | solution.py:27
  161.8 8.4 %convolution_convert_fusion = bf16[512,1280]{1,0:T(8,128)(2,1)S(1)} fusion(bf16[512,4096]{1,0:T(8,128)(2,1)S(1)} %bitcast.111, bf16[4096,1280]{1,0:T(8,128)(2,1)} %constant_dynamic-update-slice_fusion.4), kind=kOutput, calls=%fused_computation.26 | convolution fusion | flops 5369364480 | bytes 15990784 | tf_op jit(solution)/shard_map/dot_general | solution.py:108
  178.3 4.8 %collective-permute-done.16 = bf16[128,256]{1,0:T(8,128)(2,1)S(1)} collective-permute-done((bf16[128,256]{1,0:T(8,128)(2,1)}, bf16[128,256]{1,0:T(8,128)(2,1)S(1)}, u32[]{:S(2)}, u32[]{:S(2)}) %collective-permute-start.16) | collective-permute-done | bytes 65568 | tf_op jit(solution)/shard_map/ppermute | solution.py:76
  184.7 82.0 %all-gather.7.cloned.1.call-done = bf16[8192,512]{1,0:T(8,128)(2,1)} async-done(((bf16[512,512]{1,0:T(8,128)(2,1)}), bf16[8192,512]{1,0:T(8,128)(2,1)}) %all-gather.7.cloned.1.call-update) | async-done | bytes 8388624 | tf_op jit(solution)/shard_map/all_gather | solution.py:61
  266.7 5.7 %fusion.39 = (bf16[8192,256]{1,0:T(8,128)(2,1)}, bf16[8192,256]{1,0:T(8,128)(2,1)}) fusion(bf16[8192,512]{1,0:T(8,128)(2,1)} %all-gather.7.cloned.1.call-done), kind=kLoop, calls=%fused_computation.89 | loop fusion | bytes 16777216 | tf_op jit(solution)/shard_map/slice | solution.py:63
  272.4 6.9 %reshape.210 = bf16[8,1024,1,2,128]{4,3,1,0,2:T(2,128)(2,1)} reshape(bf16[8192,256]{1,0:T(8,128)(2,1)} %get-tuple-element.116) | data formatting | bytes 8388608 | tf_op jit(solution)/shard_map/reshape | solution.py:128
  279.3 76.2 %while.15 = (s32[]{:T(128)}, f32[1,2,512]{2,1,0:T(2,128)S(1)}, f32[1,2,512]{2,1,0:T(2,128)S(1)}, f32[1,2,512,256]{3,2,1,0:T(8,128)}, bf16[8,1024,1,2,128]{4,3,1,...) while((s32[]{:T(128)}, f32[1,2,512]{2,1,0:T(2,128)S(1)}, ...), condition=%wide.region_4.5_spmd.clone, body=%wide.region_1.4_spmd.clone.sunk | while | flops 814487552 | bytes 33882760 | solution.py:150
  283.5 4.3 %fusion.56 = f32[1,2,512,256]{3,2,1,0:T(8,128)} fusion(f32[2,1024,512]{2,1,0:T(8,128)} %get-tuple-element.175, f32[2,512]{1,0:T(2,128)S(1)} %bitcast.115, f32[1,2,512,256]{3,2,1,0:T(8,128)} %get-tuple-element.189, bf16[8,1024,1,256]{3,1,2,0:T(8,128)(2,1)} %get-tuple-element.201, s32[]{:T(128)} %get-tuple-element.186, ...), kind=kOutput, calls=%fused_computation.9.clone.1 | convolution fusion | flops 540803072 | bytes 6824449 | tf_op jit(solution)/shard_map/while/body/eval_jaxpr/hmqk,khe->hmqe/dot_general | solution.py:142
  292.7 4.7 %fusion.56 = f32[1,2,512,256]{3,2,1,0:T(8,128)} fusion(f32[2,1024,512]{2,1,0:T(8,128)} %get-tuple-element.175, f32[2,512]{1,0:T(2,128)S(1)} %bitcast.115, f32[1,2,512,256]{3,2,1,0:T(8,128)} %get-tuple-element.189, bf16[8,1024,1,256]{3,1,2,0:T(8,128)(2,1)} %get-tuple-element.201, s32[]{:T(128)} %get-tuple-element.186, ...), kind=kOutput, calls=%fused_computation.9.clone.1 | convolution fusion | flops 540803072 | bytes 6824449 | tf_op jit(solution)/shard_map/while/body/eval_jaxpr/hmqk,khe->hmqe/dot_general | solution.py:142
  302.3 4.7 %fusion.56 = f32[1,2,512,256]{3,2,1,0:T(8,128)} fusion(f32[2,1024,512]{2,1,0:T(8,128)} %get-tuple-element.175, f32[2,512]{1,0:T(2,128)S(1)} %bitcast.115, f32[1,2,512,256]{3,2,1,0:T(8,128)} %get-tuple-element.189, bf16[8,1024,1,256]{3,1,2,0:T(8,128)(2,1)} %get-tuple-element.201, s32[]{:T(128)} %get-tuple-element.186, ...), kind=kOutput, calls=%fused_computation.9.clone.1 | convolution fusion | flops 540803072 | bytes 6824449 | tf_op jit(solution)/shard_map/while/body/eval_jaxpr/hmqk,khe->hmqe/dot_general | solution.py:142
  311.8 4.7 %fusion.56 = f32[1,2,512,256]{3,2,1,0:T(8,128)} fusion(f32[2,1024,512]{2,1,0:T(8,128)} %get-tuple-element.175, f32[2,512]{1,0:T(2,128)S(1)} %bitcast.115, f32[1,2,512,256]{3,2,1,0:T(8,128)} %get-tuple-element.189, bf16[8,1024,1,256]{3,1,2,0:T(8,128)(2,1)} %get-tuple-element.201, s32[]{:T(128)} %get-tuple-element.186, ...), kind=kOutput, calls=%fused_computation.9.clone.1 | convolution fusion | flops 540803072 | bytes 6824449 | tf_op jit(solution)/shard_map/while/body/eval_jaxpr/hmqk,khe->hmqe/dot_general | solution.py:142
  321.4 4.7 %fusion.56 = f32[1,2,512,256]{3,2,1,0:T(8,128)} fusion(f32[2,1024,512]{2,1,0:T(8,128)} %get-tuple-element.175, f32[2,512]{1,0:T(2,128)S(1)} %bitcast.115, f32[1,2,512,256]{3,2,1,0:T(8,128)} %get-tuple-element.189, bf16[8,1024,1,256]{3,1,2,0:T(8,128)(2,1)} %get-tuple-element.201, s32[]{:T(128)} %get-tuple-element.186, ...), kind=kOutput, calls=%fused_computation.9.clone.1 | convolution fusion | flops 540803072 | bytes 6824449 | tf_op jit(solution)/shard_map/while/body/eval_jaxpr/hmqk,khe->hmqe/dot_general | solution.py:142
  331.0 4.7 %fusion.56 = f32[1,2,512,256]{3,2,1,0:T(8,128)} fusion(f32[2,1024,512]{2,1,0:T(8,128)} %get-tuple-element.175, f32[2,512]{1,0:T(2,128)S(1)} %bitcast.115, f32[1,2,512,256]{3,2,1,0:T(8,128)} %get-tuple-element.189, bf16[8,1024,1,256]{3,1,2,0:T(8,128)(2,1)} %get-tuple-element.201, s32[]{:T(128)} %get-tuple-element.186, ...), kind=kOutput, calls=%fused_computation.9.clone.1 | convolution fusion | flops 540803072 | bytes 6824449 | tf_op jit(solution)/shard_map/while/body/eval_jaxpr/hmqk,khe->hmqe/dot_general | solution.py:142
  340.6 4.7 %fusion.56 = f32[1,2,512,256]{3,2,1,0:T(8,128)} fusion(f32[2,1024,512]{2,1,0:T(8,128)} %get-tuple-element.175, f32[2,512]{1,0:T(2,128)S(1)} %bitcast.115, f32[1,2,512,256]{3,2,1,0:T(8,128)} %get-tuple-element.189, bf16[8,1024,1,256]{3,1,2,0:T(8,128)(2,1)} %get-tuple-element.201, s32[]{:T(128)} %get-tuple-element.186, ...), kind=kOutput, calls=%fused_computation.9.clone.1 | convolution fusion | flops 540803072 | bytes 6824449 | tf_op jit(solution)/shard_map/while/body/eval_jaxpr/hmqk,khe->hmqe/dot_general | solution.py:142
  350.1 4.7 %fusion.56 = f32[1,2,512,256]{3,2,1,0:T(8,128)} fusion(f32[2,1024,512]{2,1,0:T(8,128)} %get-tuple-element.175, f32[2,512]{1,0:T(2,128)S(1)} %bitcast.115, f32[1,2,512,256]{3,2,1,0:T(8,128)} %get-tuple-element.189, bf16[8,1024,1,256]{3,1,2,0:T(8,128)(2,1)} %get-tuple-element.201, s32[]{:T(128)} %get-tuple-element.186, ...), kind=kOutput, calls=%fused_computation.9.clone.1 | convolution fusion | flops 540803072 | bytes 6824449 | tf_op jit(solution)/shard_map/while/body/eval_jaxpr/hmqk,khe->hmqe/dot_general | solution.py:142
  362.1 42.3 %reduce-scatter.2.cloned.1.call-done = bf16[64,4096]{1,0:T(8,128)(2,1)} async-done(((bf16[512,4096]{1,0:T(8,128)(2,1)}), bf16[64,4096]{1,0:T(8,128)(2,1)}) %reduce-scatter.2.cloned.1.call-update) | async-done | bytes 524304 | tf_op jit(solution)/shard_map/reduce_scatter | solution.py:189
  (167 shorter events, 122.5 us)
Async XLA Ops:
  6.5 350.6 %copy-start = (bf16[256,4096]{1,0:T(8,128)(2,1)S(1)}, bf16[256,4096]{1,0:T(8,128)(2,1)}, u32[]{:S(2)}) copy-start(bf16[256,4096]{1,0:T(8,128)(2,1)} %param.24) | copy-start | bytes 6291460
  6.6 62.9 %all-gather.9.cloned.1.call-start = ((), (), s32[]{:S(2)}) async-start(), calls=%async_computation.4 | async-start | bytes 2621440 | tf_op jit(solution)/shard_map/all_gather | solution.py:48
  10.1 149.3 %all-gather.5.cloned.1.call-start = ((), (), s32[]{:S(2)}) async-start(), calls=%async_computation.1 | async-start | bytes 6291456 | tf_op jit(solution)/shard_map/all_gather | solution.py:48
  14.8 37.3 %collective-permute-start = (bf16[256,1280]{1,0:T(8,128)(2,1)S(1)}, bf16[256,1280]{1,0:T(8,128)(2,1)S(1)}, u32[]{:S(2)}, u32[]{:S(2)}) collective-permute-start(bf16[256,1280]{1,0:T(8,128)(2,1)S(1)} %bitcast_dynamic-update-slice_fusion), channel_id=1, source_target_pairs={{0,8},{8,16},{16,24},{24,32},{32,40},{40,48},{48,56},{56,64},{64,7... | collective-permute-start | bytes 1966088 | tf_op jit(solution)/shard_map/ppermute | solution.py:27
  17.6 34.4 %collective-permute-start.1 = (bf16[256,1280]{1,0:T(8,128)(2,1)S(1)}, bf16[256,1280]{1,0:T(8,128)(2,1)}, u32[]{:S(2)}, u32[]{:S(2)}) collective-permute-start(bf16[256,1280]{1,0:T(8,128)(2,1)S(1)} %bitcast_dynamic-update-slice_fusion), channel_id=1, source_target_pairs={{0,120},{8,0},{16,8},{24,16},{32,24},{40,32},{48,40},{56,48},{64,5... | collective-permute-start | bytes 1966088 | tf_op jit(solution)/shard_map/ppermute | solution.py:32
  52.1 17.4 %collective-permute-start.2 = (bf16[256,1280]{1,0:T(8,128)(2,1)S(1)}, bf16[256,1280]{1,0:T(8,128)(2,1)}, u32[]{:S(2)}, u32[]{:S(2)}) collective-permute-start(bf16[256,1280]{1,0:T(8,128)(2,1)S(1)} %collective-permute-done), channel_id=1, source_target_pairs={{0,8},{8,16},{16,24},{24,32},{32,40},{40,48},{48,56},{56,64},{64,7... | collective-permute-start | bytes 1966088 | tf_op jit(solution)/shard_map/ppermute | solution.py:27
  52.1 17.5 %collective-permute-start.3 = (bf16[256,1280]{1,0:T(8,128)(2,1)}, bf16[256,1280]{1,0:T(8,128)(2,1)}, u32[]{:S(2)}, u32[]{:S(2)}) collective-permute-start(bf16[256,1280]{1,0:T(8,128)(2,1)} %collective-permute-done.1), channel_id=1, source_target_pairs={{0,120},{8,0},{16,8},{24,16},{32,24},{40,32},{48,40},{56,48},{64,5... | collective-permute-start | bytes 1966088 | tf_op jit(solution)/shard_map/ppermute | solution.py:32
  69.4 16.6 %collective-permute-start.4 = (bf16[256,1280]{1,0:T(8,128)(2,1)}, bf16[256,1280]{1,0:T(8,128)(2,1)S(1)}, u32[]{:S(2)}, u32[]{:S(2)}) collective-permute-start(bf16[256,1280]{1,0:T(8,128)(2,1)} %collective-permute-done.2), channel_id=1, source_target_pairs={{0,8},{8,16},{16,24},{24,32},{32,40},{40,48},{48,56},{56,64},{64,7... | collective-permute-start | bytes 1966088 | tf_op jit(solution)/shard_map/ppermute | solution.py:27
  69.5 197.2 %all-gather.7.cloned.1.call-start = ((), (), s32[]{:S(2)}) async-start(), calls=%async_computation.2 | async-start | bytes 8912896 | tf_op jit(solution)/shard_map/all_gather | solution.py:61
  69.6 23.0 %collective-permute-start.5 = (bf16[256,1280]{1,0:T(8,128)(2,1)}, bf16[256,1280]{1,0:T(8,128)(2,1)}, u32[]{:S(2)}, u32[]{:S(2)}) collective-permute-start(bf16[256,1280]{1,0:T(8,128)(2,1)} %collective-permute-done.3), channel_id=1, source_target_pairs={{0,120},{8,0},{16,8},{24,16},{32,24},{40,32},{48,40},{56,48},{64,5... | collective-permute-start | bytes 1966088 | tf_op jit(solution)/shard_map/ppermute | solution.py:32
  72.9 18.7 %copy-start.5 = (bf16[256,1280]{1,0:T(8,128)(2,1)S(1)}, bf16[256,1280]{1,0:T(8,128)(2,1)}, u32[]{:S(2)}) copy-start(bf16[256,1280]{1,0:T(8,128)(2,1)} %copy-done.4) | copy-start | bytes 1966084
  86.1 15.6 %collective-permute-start.6 = (bf16[256,1280]{1,0:T(8,128)(2,1)S(1)}, bf16[256,1280]{1,0:T(8,128)(2,1)S(1)}, u32[]{:S(2)}, u32[]{:S(2)}) collective-permute-start(bf16[256,1280]{1,0:T(8,128)(2,1)S(1)} %collective-permute-done.4), channel_id=1, source_target_pairs={{0,8},{8,16},{16,24},{24,32},{32,40},{40,48},{48,56},{56,64},{64,7... | collective-permute-start | bytes 1966088 | tf_op jit(solution)/shard_map/ppermute | solution.py:27
  92.6 15.1 %collective-permute-start.7 = (bf16[256,1280]{1,0:T(8,128)(2,1)}, bf16[256,1280]{1,0:T(8,128)(2,1)S(1)}, u32[]{:S(2)}, u32[]{:S(2)}) collective-permute-start(bf16[256,1280]{1,0:T(8,128)(2,1)} %collective-permute-done.5), channel_id=1, source_target_pairs={{0,120},{8,0},{16,8},{24,16},{32,24},{40,32},{48,40},{56,48},{64,5... | collective-permute-start | bytes 1966088 | tf_op jit(solution)/shard_map/ppermute | solution.py:32
  101.6 14.9 %collective-permute-start.8 = (bf16[256,1280]{1,0:T(8,128)(2,1)S(1)}, bf16[256,1280]{1,0:T(8,128)(2,1)S(1)}, u32[]{:S(2)}, u32[]{:S(2)}) collective-permute-start(bf16[256,1280]{1,0:T(8,128)(2,1)S(1)} %collective-permute-done.6), channel_id=1, source_target_pairs={{0,8},{8,16},{16,24},{24,32},{32,40},{40,48},{48,56},{56,64},{64,7... | collective-permute-start | bytes 1966088 | tf_op jit(solution)/shard_map/ppermute | solution.py:27
  107.7 14.8 %collective-permute-start.9 = (bf16[256,1280]{1,0:T(8,128)(2,1)S(1)}, bf16[256,1280]{1,0:T(8,128)(2,1)S(1)}, u32[]{:S(2)}, u32[]{:S(2)}) collective-permute-start(bf16[256,1280]{1,0:T(8,128)(2,1)S(1)} %collective-permute-done.7), channel_id=1, source_target_pairs={{0,120},{8,0},{16,8},{24,16},{32,24},{40,32},{48,40},{56,48},{64,5... | collective-permute-start | bytes 1966088 | tf_op jit(solution)/shard_map/ppermute | solution.py:32
  116.5 14.9 %collective-permute-start.10 = (bf16[256,1280]{1,0:T(8,128)(2,1)S(1)}, bf16[256,1280]{1,0:T(8,128)(2,1)S(1)}, u32[]{:S(2)}, u32[]{:S(2)}) collective-permute-start(bf16[256,1280]{1,0:T(8,128)(2,1)S(1)} %collective-permute-done.8), channel_id=1, source_target_pairs={{0,8},{8,16},{16,24},{24,32},{32,40},{40,48},{48,56},{56,64},{64,7... | collective-permute-start | bytes 1966088 | tf_op jit(solution)/shard_map/ppermute | solution.py:27
  122.5 14.9 %collective-permute-start.11 = (bf16[256,1280]{1,0:T(8,128)(2,1)S(1)}, bf16[256,1280]{1,0:T(8,128)(2,1)S(1)}, u32[]{:S(2)}, u32[]{:S(2)}) collective-permute-start(bf16[256,1280]{1,0:T(8,128)(2,1)S(1)} %collective-permute-done.9), channel_id=1, source_target_pairs={{0,120},{8,0},{16,8},{24,16},{32,24},{40,32},{48,40},{56,48},{64,5... | collective-permute-start | bytes 1966088 | tf_op jit(solution)/shard_map/ppermute | solution.py:32
  131.4 14.9 %collective-permute-start.12 = (bf16[256,1280]{1,0:T(8,128)(2,1)S(1)}, bf16[256,1280]{1,0:T(8,128)(2,1)S(1)}, u32[]{:S(2)}, u32[]{:S(2)}) collective-permute-start(bf16[256,1280]{1,0:T(8,128)(2,1)S(1)} %collective-permute-done.10), channel_id=1, source_target_pairs={{0,8},{8,16},{16,24},{24,32},{32,40},{40,48},{48,56},{56,64},{64,7... | collective-permute-start | bytes 1966088 | tf_op jit(solution)/shard_map/ppermute | solution.py:27
  137.4 12.7 %collective-permute-start.13 = (bf16[256,1280]{1,0:T(8,128)(2,1)S(1)}, bf16[256,1280]{1,0:T(8,128)(2,1)S(1)}, u32[]{:S(2)}, u32[]{:S(2)}) collective-permute-start(bf16[256,1280]{1,0:T(8,128)(2,1)S(1)} %collective-permute-done.11), channel_id=1, source_target_pairs={{0,120},{8,0},{16,8},{24,16},{32,24},{40,32},{48,40},{56,48},{64,5... | collective-permute-start | bytes 1966088 | tf_op jit(solution)/shard_map/ppermute | solution.py:32
  146.3 12.1 %collective-permute-start.14 = (bf16[256,1280]{1,0:T(8,128)(2,1)S(1)}, bf16[256,1280]{1,0:T(8,128)(2,1)S(1)}, u32[]{:S(2)}, u32[]{:S(2)}) collective-permute-start(bf16[256,1280]{1,0:T(8,128)(2,1)S(1)} %collective-permute-done.12), channel_id=1, source_target_pairs={{0,8},{8,16},{16,24},{24,32},{32,40},{40,48},{48,56},{56,64},{64,7... | collective-permute-start | bytes 1966088 | tf_op jit(solution)/shard_map/ppermute | solution.py:27
  171.3 233.1 %reduce-scatter.2.cloned.1.call-start = ((), (), s32[]{:S(2)}) async-start(), calls=%async_computation.3 | async-start | bytes 4718592 | tf_op jit(solution)/shard_map/reduce_scatter | solution.py:189
  173.8 4.5 %collective-permute-start.15 = (bf16[128,256]{1,0:T(8,128)(2,1)}, bf16[128,256]{1,0:T(8,128)(2,1)S(1)}, u32[]{:S(2)}, u32[]{:S(2)}) collective-permute-start(bf16[128,256]{1,0:T(8,128)(2,1)} %get-tuple-element.120), channel_id=1, source_target_pairs={{0,8},{8,16},{16,24},{24,32},{32,40},{40,48},{48,56},{56,64},{64,7... | collective-permute-start | bytes 196616 | tf_op jit(solution)/shard_map/ppermute | solution.py:75
  175.3 7.9 %collective-permute-start.16 = (bf16[128,256]{1,0:T(8,128)(2,1)}, bf16[128,256]{1,0:T(8,128)(2,1)S(1)}, u32[]{:S(2)}, u32[]{:S(2)}) collective-permute-start(bf16[128,256]{1,0:T(8,128)(2,1)} %get-tuple-element.121), channel_id=1, source_target_pairs={{8,0},{16,8},{24,16},{32,24},{40,32},{48,40},{56,48},{64,56},{72,6... | collective-permute-start | bytes 196616 | tf_op jit(solution)/shard_map/ppermute | solution.py:76
  279.3 77.9 %copy-start.7 = (f32[256]{0:T(256)S(1)}, f32[256]{0:T(256)}, u32[]{:S(2)}) copy-start(f32[256]{0:T(256)} %param.20) | copy-start | bytes 3076
  (13 other events, 63.2 us)
Sparse Core Ops, SparseCore 0:
  10.2 50.0 all-gather.8
  69.6 17.3 all-gather.4
  171.4 95.2 all-gather.6
  362.2 42.0 reduce-scatter.1
